TPU v7x, 32 devices: a whole 2x2x4 slice. The times are simulated.
32 devices in a mesh: kv: 4 (over y, x), tp: 8 (over z, core).
Axes of the slice: x: 2, y: 2, z: 4, core: 2. Of those that a mesh axis runs over, the one named last changes fastest.
Arguments:
- tokens: bfloat16 [3, 4096], P(None, ('kv', 'tp')), may hold values from -40 to 40
- lengths: int32 [3], replicated, may hold values from 1 to 8192, as said below
- attn_gain: float32 [4096], P(('kv', 'tp')), may hold values from 0.1 to 1.9
- w_query: bfloat16 [4096, 2048], P('kv', 'tp'), may hold values from -0.09375 to 0.09375
- w_key: bfloat16 [4096, 128], P('kv'), may hold values from -0.09375 to 0.09375
- w_value: bfloat16 [4096, 128], P('kv'), may hold values from -0.09375 to 0.09375
- w_forget: bfloat16 [4096, 32], replicated, may hold values from -0.09375 to 0.09375
- forget_bias: float32 [32], replicated, may hold values from -4 to 0
- cache_keys: bfloat16 [3, 128, 8192], P(None, None, ('kv', 'tp')), may hold values from -320 to 320
- cache_values: bfloat16 [3, 128, 8192], P(None, None, ('kv', 'tp')), may hold values from -6 to 6
- cache_decay: float32 [3, 32, 8192], P(None, None, ('kv', 'tp')), may hold values from -1028 to 0, as said below
- out_gain: float32 [2048], replicated, may hold values from 0.1 to 1.9
- w_out: bfloat16 [2048, 4096], P('tp', 'kv'), may hold values from -0.125 to 0.125
- mlp_gain: float32 [4096], P(('kv', 'tp')), may hold values from 0.1 to 1.9
- w_gate: bfloat16 [4096, 11264], P('kv', 'tp'), may hold values from -0.09375 to 0.09375
- w_up: bfloat16 [4096, 11264], P('kv', 'tp'), may hold values from -0.09375 to 0.09375
- w_down: bfloat16 [11264, 4096], P('tp', 'kv'), may hold values from -0.0546875 to 0.0546875
Outputs:
- layer_out: bfloat16 [3, 4096], P(None, ('kv', 'tp'))
Inputs may be any that keep to these rules, and one draw needn't show every extreme that they name: Sequence b has lengths[b] live cache positions, 0 to lengths[b] - 1; some sequence has exactly 8192 in every draw. On live positions, cache_decay[b, h, j] is the sum of the log forget gates of sequence b and head h over positions j + 1 to lengths[b] - 1, so it is zero at the last live position and never rises toward earlier positions; it is zero beyond lengths[b].
All inputs are finite; a program needn't handle non-finite values.
Results may differ from a plain program's by a relative error of at most 0.013.
Values may be sent and summed in bfloat16 or wider, within the bound.
A program may use at most 64 MiB of HBM per device.

v0:
```python
import jax
import jax.numpy as jnp
from jax import lax
from jax.sharding import PartitionSpec as P

QUERY_HEAD_COUNT = 32
HD = 64
KV_HEADS = 2
epsilon = 1e-06
masked_score = -1e30


def spread_rows(share, gain):
    scaled = (share.astype(jnp.float32) * gain).astype(jnp.bfloat16)
    squares = jnp.sum(jnp.square(share.astype(jnp.float32)), axis=1)
    row_block = lax.all_gather(scaled, "tp", axis=1, tiled=True)
    square_total = lax.psum(squares, ("kv", "tp"))
    return (row_block, square_total)


def body(
    tokens,
    lengths,
    attn_gain,
    w_query,
    w_key,
    w_value,
    w_forget,
    forget_bias,
    cache_keys,
    cache_values,
    cache_decay,
    out_gain,
    w_out,
    mlp_gain,
    w_gate,
    w_up,
    w_down,
):
    full_width = tokens.shape[1] * lax.axis_size("kv") * lax.axis_size("tp")
    kv_index = lax.axis_index("kv")
    tp_index = lax.axis_index("tp")
    row_block, square_total = spread_rows(tokens, attn_gain)
    block_rows = row_block.shape[1]
    forget_rows = lax.dynamic_slice_in_dim(w_forget, kv_index * block_rows, block_rows, 0)
    query_part = jnp.dot(row_block, w_query, preferred_element_type=jnp.float32)
    key_part = jnp.dot(row_block, w_key, preferred_element_type=jnp.float32)
    value_part = jnp.dot(row_block, w_value, preferred_element_type=jnp.float32)
    forget_part = jnp.dot(row_block, forget_rows, preferred_element_type=jnp.float32)
    query_sum, key_sum, value_sum, forget_sum = lax.psum(
        (query_part, key_part, value_part, forget_part), "kv"
    )
    first_rms = lax.rsqrt(square_total / full_width + epsilon)[:, None]
    query_local = (query_sum * first_rms).astype(jnp.bfloat16)
    key_new = (key_sum * first_rms).astype(jnp.bfloat16)
    value_new = (value_sum * first_rms).astype(jnp.bfloat16)
    log_gate = jax.nn.log_sigmoid(forget_sum * first_rms + forget_bias)
    query_all = lax.all_gather(query_local, "tp", axis=1, tiled=True)
    batch_rows, key_dims, span = cache_keys.shape
    groups = QUERY_HEAD_COUNT // KV_HEADS
    score_scale = HD ** (-0.5)
    query_grouped = query_all.reshape(batch_rows, KV_HEADS, groups, HD)
    keys_grouped = cache_keys.reshape(batch_rows, KV_HEADS, HD, span)
    values_grouped = cache_values.reshape(batch_rows, KV_HEADS, HD, span)
    scores = jnp.einsum(
        "bkgd,bkdj->bkgj", query_grouped, keys_grouped, preferred_element_type=jnp.float32
    ).reshape(batch_rows, QUERY_HEAD_COUNT, span)
    scores = scores * score_scale + cache_decay + log_gate[:, :, None]
    first_slot = (kv_index * lax.axis_size("tp") + tp_index) * span
    token_positions = first_slot + lax.iota(jnp.int32, span)
    is_live = (token_positions[None, :] < lengths[:, None])[:, None, :]
    scores = jnp.where(is_live, scores, masked_score)
    own_score = (
        jnp.einsum(
            "inpo,ino->inp",
            query_grouped,
            key_new.reshape(batch_rows, KV_HEADS, HD),
            preferred_element_type=jnp.float32,
        ).reshape(batch_rows, QUERY_HEAD_COUNT)
        * score_scale
    )
    local_top = jnp.maximum(jnp.max(scores, axis=2), own_score)
    head_count = w_out.shape[0] // HD
    head_start = tp_index * head_count
    score_top = lax.pmax(local_top, ("kv", "tp"))
    weights = jnp.where(is_live, jnp.exp(scores - score_top[:, :, None]), 0.0)
    weight_total = jnp.sum(weights, axis=2)
    rounded = weights.astype(jnp.bfloat16).reshape(batch_rows, KV_HEADS, groups, span)
    value_sums = jnp.einsum(
        "bkgj,bkdj->bkgd", rounded, values_grouped, preferred_element_type=jnp.float32
    ).reshape(batch_rows, QUERY_HEAD_COUNT, HD)
    weight_total, value_sums = (weight_total, value_sums)
    weight_total, value_sums = (
        lax.psum_scatter(weight_total, "tp", scatter_dimension=1, tiled=True),
        lax.psum_scatter(value_sums, "tp", scatter_dimension=1, tiled=True),
    )
    weight_total, value_sums = lax.psum((weight_total, value_sums), "kv")
    score_top = lax.dynamic_slice_in_dim(score_top, head_start, head_count, 1)
    own_here = lax.dynamic_slice_in_dim(own_score, head_start, head_count, 1)
    new_values = jnp.repeat(value_new.reshape(batch_rows, KV_HEADS, HD), groups, axis=1)
    new_values = lax.dynamic_slice_in_dim(new_values, head_start, head_count, 1).astype(jnp.float32)
    own_weight = jnp.exp(own_here - score_top)
    heads_out = (value_sums + own_weight[:, :, None] * new_values) / (weight_total + own_weight)[
        :, :, None
    ]
    head_gains = lax.dynamic_slice_in_dim(out_gain, head_start * HD, head_count * HD, 0).reshape(
        head_count, HD
    )
    normed = (
        heads_out
        * lax.rsqrt(jnp.mean(jnp.square(heads_out), axis=2, keepdims=True) + epsilon)
        * head_gains
    )
    normed = normed.astype(jnp.bfloat16).reshape(batch_rows, head_count * HD)
    attn_part = jnp.dot(normed, w_out, preferred_element_type=jnp.float32)
    attn_share = lax.psum_scatter(attn_part, "tp", scatter_dimension=1, tiled=True)
    residual = (tokens.astype(jnp.float32) + attn_share).astype(jnp.bfloat16)
    mlp_block, mlp_squares = spread_rows(residual, mlp_gain)
    gate_part = jnp.dot(mlp_block, w_gate, preferred_element_type=jnp.float32)
    up_part = jnp.dot(mlp_block, w_up, preferred_element_type=jnp.float32)
    gate_sum, up_sum = lax.psum((gate_part, up_part), "kv")
    second_rms = lax.rsqrt(mlp_squares / full_width + epsilon)[:, None]
    hidden = (jax.nn.silu(gate_sum * second_rms) * (up_sum * second_rms)).astype(jnp.bfloat16)
    down_part = jnp.dot(hidden, w_down, preferred_element_type=jnp.float32)
    mlp_share = lax.psum_scatter(down_part, "tp", scatter_dimension=1, tiled=True)
    return (residual.astype(jnp.float32) + mlp_share).astype(jnp.bfloat16)


def solution(mesh):
    placed = (
        P(None, ("kv", "tp")),
        P(),
        P(("kv", "tp")),
        P("kv", "tp"),
        P("kv", None),
        P("kv", None),
        P(),
        P(),
        P(None, None, ("kv", "tp")),
        P(None, None, ("kv", "tp")),
        P(None, None, ("kv", "tp")),
        P(),
        P("tp", "kv"),
        P(("kv", "tp")),
        P("kv", "tp"),
        P("kv", "tp"),
        P("tp", "kv"),
    )
    return jax.shard_map(
        body, mesh=mesh, in_specs=placed, out_specs=P(None, ("kv", "tp")), check_vma=False
    )
```

profile of v0, /device:TPU:0, one launch (start us, length us, event | category | flops | bytes accessed | tf_op | source)
XLA Modules:
  0.0 321.7 jit_solution(4829693310829404246)
XLA Ops:
  6.5 0.9 dynamic_slice.19
  7.5 0.7 mul.150
  8.2 0.8 fusion.11
  8.9 42.0 %psum.71 = f32[3]{0:T(128)S(1)} all-reduce(f32[3]{0:T(128)S(1)} %get-tuple-element.23), channel_id=1, replica_groups=mesh['kv'=4,'tp'=8] {'kv','tp'}, use_global_device_ids=true, to_apply=%region_2.0 | all-reduce | flops 3 | bytes 24 | tf_op jit(solution)/shard_map/psum | solution.py:17
  51.0 10.6 %all_gather.9 = bf16[3,1024]{1,0:T(4,128)(2,1)S(1)} all-gather(bf16[3,128]{1,0:T(4,128)(2,1)S(1)} %get-tuple-element.24), channel_id=1, replica_groups=mesh['kv'=4,'tp'=8] {'tp'}, dimensions={1}, use_global_device_ids=true | all-gather | bytes 6912 | tf_op jit(solution)/shard_map/all_gather | solution.py:16
  61.5 1.7 fusion.25
  63.2 1.1 fusion.22
  64.3 1.2 fusion.21
  65.5 1.0 fusion.3
  66.5 9.9 %all-reduce.5 = (f32[3,256]{1,0:T(4,128)S(1)}, f32[3,32]{1,0:T(4,128)S(1)}, f32[3,128]{1,0:T(4,128)S(1)}) all-reduce(f32[3,256]{1,0:T(4,128)S(1)} %fusion.21, f32[3,32]{1,0:T(4,128)S(1)} %fusion.3, f32[3,128]{1,0:T(4,128)S(1)} %fusion.22), channel_id=1, replica_groups=mesh['kv'=4,'tp'=8] {'kv'}, use_global_device_ids=true, to_apply=%region_0.0 | all-reduce | flops 1248 | bytes 9984 | tf_op jit(solution)/shard_map/psum | solution.py:50
  76.4 0.1 multiply_convert_fusion.1
  76.5 0.1 reshape.90
  76.6 12.8 %all_gather.10 = bf16[3,2048]{1,0:T(4,128)(2,1)S(1)} all-gather(bf16[3,256]{1,0:T(4,128)(2,1)S(1)} %multiply_convert_fusion.1), channel_id=1, replica_groups=mesh['kv'=4,'tp'=8] {'tp'}, dimensions={1}, use_global_device_ids=true | all-gather | bytes 13824 | tf_op jit(solution)/shard_map/all_gather | solution.py:58
  89.4 0.1 reshape.78
  89.5 0.1 fusion.23
  89.6 0.1 mul.142
  89.7 1.1 convolution_multiply_fusion
  90.8 0.7 broadcast_compare_fusion
  91.5 0.7 fusion.16
  92.2 1.0 fusion
  93.2 0.1 select_reduce_fusion
  93.4 37.8 %pmax.7 = f32[3,32]{1,0:T(4,128)} all-reduce(f32[3,32]{1,0:T(4,128)S(1)} %max.17), channel_id=1, replica_groups=mesh['kv'=4,'tp'=8] {'kv','tp'}, use_global_device_ids=true, to_apply=%region_6.7 | all-reduce | flops 96 | bytes 768 | tf_op jit(solution)/shard_map/pmax | solution.py:85
  131.2 1.4 fusion.1
  132.6 1.2 dynamic-slice
  134.5 1.1 fusion.24
  135.6 27.4 %all-reduce.2 = (f32[3,32,64]{2,1,0:T(8,128)S(1)}, f32[3,32]{1,0:T(4,128)S(1)}) all-reduce(f32[3,32,64]{2,1,0:T(8,128)S(1)} %bitcast.42, f32[3,32]{1,0:T(4,128)} %get-tuple-element.21), channel_id=2, replica_groups=mesh['kv'=4,'tp'=8] {'tp'}, use_global_device_ids=true, to_apply=%region_7.8.clone | all-reduce | flops 6240 | bytes 49920
  163.0 0.1 constant_dynamic-slice_fusion
  163.1 16.6 %all-reduce.4 = (f32[3,4,64]{2,1,0:T(4,128)S(1)}, f32[3,4]{1,0:T(4,128)S(1)}, f32[3,128]{1,0:T(4,128)S(1)}) all-reduce(f32[3,4,64]{2,1,0:T(4,128)S(1)} %constant_dynamic-slice_fusion.1, f32[3,4]{1,0:T(4,128)S(1)} %constant_dynamic-slice_fusion, f32[3,128]{1,0:T(4,128)} %fusion.25), channel_id=1, replica_groups=mesh['kv'=4,'tp'=8] {'kv'}, use_global_device_ids=true, to_apply=%region_8.9 | all-reduce | flops 1164 | bytes 9312 | tf_op jit(solution)/shard_map/psum | solution.py:97
  179.7 0.7 multiply_convert_fusion.2
  180.4 0.1 reshape.84
  180.5 0.8 fusion.20
  181.2 0.2 multiply_reduce_fusion
  181.4 0.8 multiply_convert_fusion
  182.2 0.1 reshape.86
  182.3 1.1 convolution_bitcast_fusion.1
  183.5 27.8 %reduce-scatter.9.cloned.1.call-done = f32[128,3]{1,0:T(8,128)} async-done(((f32[1024,3]{1,0:T(8,128)}), f32[128,3]{1,0:T(8,128)}) %reduce-scatter.9.cloned.1.call-update) | async-done | bytes 1552
  211.3 0.9 copy.24
  212.2 0.8 fusion.14
  213.0 37.8 %psum.78 = f32[3]{0:T(128)S(1)} all-reduce(f32[3]{0:T(128)S(1)} %get-tuple-element.15), channel_id=1, replica_groups=mesh['kv'=4,'tp'=8] {'kv','tp'}, use_global_device_ids=true, to_apply=%region_17.18 | all-reduce | flops 3 | bytes 24 | tf_op jit(solution)/shard_map/psum | solution.py:17
  250.8 0.8 fusion.13
  251.6 11.4 %all_gather.11 = bf16[3,1024]{1,0:T(4,128)(2,1)S(1)} all-gather(bf16[3,128]{1,0:T(4,128)(2,1)S(1)} %fusion.13), channel_id=1, replica_groups=mesh['kv'=4,'tp'=8] {'tp'}, dimensions={1}, use_global_device_ids=true | all-gather | bytes 6912 | tf_op jit(solution)/shard_map/all_gather | solution.py:16
  263.0 0.5 fusion.27
  263.5 0.5 fusion.26
  264.0 16.7 %all-reduce.3 = (f32[3,1408]{1,0:T(4,128)S(1)}, f32[3,1408]{1,0:T(4,128)S(1)}) all-reduce(f32[3,1408]{1,0:T(4,128)S(1)} %fusion.27, f32[3,1408]{1,0:T(4,128)S(1)} %fusion.26), channel_id=1, replica_groups=mesh['kv'=4,'tp'=8] {'kv'}, use_global_device_ids=true, to_apply=%region_18.19 | all-reduce | flops 8448 | bytes 67584 | tf_op jit(solution)/shard_map/psum | solution.py:121
  280.7 3.8 %convolution_bitcast_fusion = f32[1024,3]{1,0:T(8,128)} fusion(bf16[1408,1024]{1,0:T(8,128)(2,1)} %param.33, f32[3,1408]{1,0:T(4,128)S(1)} %get-tuple-element.7, f32[3,1408]{1,0:T(4,128)S(1)} %get-tuple-element.8, f32[3]{0:T(128)S(1)} %add_rsqrt_fusion.1), kind=kOutput, calls=%fused_computation | convolution fusion | flops 8684544 | bytes 2929676
  284.5 28.8 %reduce-scatter.11.cloned.1.call-done = f32[128,3]{1,0:T(8,128)} async-done(((f32[1024,3]{1,0:T(8,128)}), f32[128,3]{1,0:T(8,128)}) %reduce-scatter.11.cloned.1.call-update) | async-done | bytes 1552
  313.3 0.9 copy.26
  314.2 0.6 fusion.15
  (25 shorter events, 0.2 us)
Async XLA Ops:
  6.5 256.5 %copy-start = (bf16[1024,1408]{1,0:T(8,128)(2,1)S(1)}, bf16[1024,1408]{1,0:T(8,128)(2,1)}, u32[]{:S(2)}) copy-start(bf16[1024,1408]{1,0:T(8,128)(2,1)} %param.32) | copy-start | bytes 8650756
  6.5 175.7 %copy-start.2 = (bf16[256,1024]{1,0:T(8,128)(2,1)S(1)}, bf16[256,1024]{1,0:T(8,128)(2,1)}, u32[]{:S(2)}) copy-start(bf16[256,1024]{1,0:T(8,128)(2,1)} %param.29) | copy-start | bytes 1572868
  6.5 204.8 %reduce-scatter.9.cloned.1.call-start = ((), (), s32[]{:S(2)}) async-start(), calls=%async_computation.2 | async-start | bytes 589824
  50.9 40.6 %copy-start.5 = (f32[3]{0:T(128)}, f32[3]{0:T(128)S(1)}, u32[]{:S(2)}) copy-start(f32[3]{0:T(128)S(1)} %add_rsqrt_fusion.2) | copy-start | bytes 40
  89.7 3.7 %copy-start.3 = (f32[3,32]{1,0:T(4,128)}, f32[3,32]{1,0:T(4,128)S(1)}, u32[]{:S(2)}) copy-start(f32[3,32]{1,0:T(4,128)S(1)} %mul.142) | copy-start | bytes 1156
  91.5 1.7 copy-start.4
  183.4 129.9 %reduce-scatter.11.cloned.1.call-start = ((), (), s32[]{:S(2)}) async-start(), calls=%async_computation.3 | async-start | bytes 589824
  250.8 12.7 %copy-start.1 = (bf16[1024,1408]{1,0:T(8,128)(2,1)S(1)}, bf16[1024,1408]{1,0:T(8,128)(2,1)}, u32[]{:S(2)}) copy-start(bf16[1024,1408]{1,0:T(8,128)(2,1)} %param.31) | copy-start | bytes 8650756
Sparse Core Ops, SparseCore 0:
  183.5 27.7 reduce-scatter.8
  284.6 28.6 reduce-scatter.10
where the time goes:
time: 323 us; the launch traced here: 322 us
  blocking collectives  223 us (69%)
  waiting for transfers between devices  56.7 us (18%)
  between operations  14.1 us (4%)
  matrix products  13.2 us (4%)
  other arithmetic  9.52 us (3%)
  local copies, waits for them, and re-layouts  5.19 us (2%)
    psum x2, blocking collectives, spread_rows(): square_total = lax.psum(squares, ('kv', 'tp'))  79.8 us
    unnamed x4, waiting for transfers between devices  56.7 us
    pmax x1, blocking collectives, body(): score_top = lax.pmax(local_top, ('kv', 'tp'))  37.8 us
    unnamed x1, blocking collectives  27.4 us
    all_gather x2, blocking collectives, spread_rows(): row_block = lax.all_gather(scaled, 'tp', axis=1, tiled=True)  22 us
    psum x1, blocking collectives, body(): gate_sum, up_sum = lax.psum((gate_part, up_part), 'kv')  16.7 us
    psum x1, blocking collectives, body(): weight_total, value_sums = lax.psum((weight_total, value_sums), 'kv')  16.6 us
    all_gather x1, blocking collectives, body(): query_all = lax.all_gather(query_local, 'tp', axis=1, tiled=True)  12.8 us
  transfers between devices with their start and end apart: 2, of which 2 were waited for; matrix products, arithmetic and copies ran while one was open for 0% of the time, Pallas kernels for 0%

commit v1 on v0

--- a/solution.py
+++ b/solution.py
@@ -13,7 +13,12 @@
 def spread_rows(share, gain):
     scaled = (share.astype(jnp.float32) * gain).astype(jnp.bfloat16)
     squares = jnp.sum(jnp.square(share.astype(jnp.float32)), axis=1)
-    row_block = lax.all_gather(scaled, "tp", axis=1, tiled=True)
+    ring = [scaled]
+    for hop in range(7):
+        ring.append(lax.ppermute(ring[-1], "tp", [(dev, (dev + 1) % 8) for dev in range(8)]))
+    row_block = jnp.roll(
+        jnp.concatenate(ring[::-1], axis=1), (lax.axis_index("tp") + 1) * ring[0].shape[1], axis=1
+    )
     square_total = lax.psum(squares, ("kv", "tp"))
     return (row_block, square_total)
 

time: 323 us -> 350 us (1.084)
  waiting for transfers between devices: 56.7 us -> 111 us
  blocking collectives: 223 us -> 200 us
  other arithmetic: 9.52 us -> 5.02 us
    ppermute x0 -> x14, waiting for transfers between devices: none -> 55.2 us  [spread_rows(): lax.ppermute(ring[-1], 'tp', [(dev, (dev + 1) % 8) for dev in range(8)])]
    all_gather x2 -> x0, blocking collectives: 22 us -> none  [spread_rows(): row_block = lax.all_gather(scaled, 'tp', axis=1, tiled=True)]
  transfers between devices with their start and end apart: 2 -> 16, of which waited for: 2 -> 14; matrix products, arithmetic and copies ran while one was open for 0% -> 1% of each run, Pallas kernels for 0% -> 0%
where the time goes in v1:
time: 350 us
  blocking collectives  200 us (57%)
  waiting for transfers between devices  111 us (32%)
  between operations  14.2 us (4%)
  matrix products  12.7 us (4%)
  local copies, waits for them, and re-layouts  5.23 us (1%)
  other arithmetic  5.02 us (1%)
    psum x2, blocking collectives, spread_rows(): square_total = lax.psum(squares, ('kv', 'tp'))  78.1 us
    unnamed x4, waiting for transfers between devices  56.1 us
    ppermute x14, waiting for transfers between devices, spread_rows(): lax.ppermute(ring[-1], 'tp', [(dev, (dev + 1) % 8) for dev in range(8)])  55.2 us
    pmax x1, blocking collectives, body(): score_top = lax.pmax(local_top, ('kv', 'tp'))  37.8 us
    unnamed x1, blocking collectives  27.8 us
    psum x1, blocking collectives, body(): gate_sum, up_sum = lax.psum((gate_part, up_part), 'kv')  17.3 us
    psum x1, blocking collectives, body(): weight_total, value_sums = lax.psum((weight_total, value_sums), 'kv')  15.8 us
    all_gather x1, blocking collectives, body(): query_all = lax.all_gather(query_local, 'tp', axis=1, tiled=True)  12.8 us
  transfers between devices with their start and end apart: 16, of which 14 were waited for; matrix products, arithmetic and copies ran while one was open for 1% of the time, Pallas kernels for 0%

profile of v1, /device:TPU:0, one launch (start us, length us, event | category | flops | bytes accessed | tf_op | source)
XLA Modules:
  0.0 349.7 jit_solution(16582781418389402827)
XLA Ops:
  6.6 1.0 fusion.13
  7.6 0.5 collective-permute-start
  8.1 5.3 %collective-permute-done = bf16[3,128]{1,0:T(4,128)(2,1)S(1)} collective-permute-done((bf16[3,128]{1,0:T(4,128)(2,1)S(1)}, bf16[3,128]{1,0:T(4,128)(2,1)S(1)}, u32[]{:S(2)}, u32[]{:S(2)}) %collective-permute-start) | collective-permute-done | bytes 800 | tf_op jit(solution)/shard_map/ppermute | solution.py:18
  13.4 4.8 %collective-permute-done.1 = bf16[3,128]{1,0:T(4,128)(2,1)S(1)} collective-permute-done((bf16[3,128]{1,0:T(4,128)(2,1)S(1)}, bf16[3,128]{1,0:T(4,128)(2,1)S(1)}, u32[]{:S(2)}, u32[]{:S(2)}) %collective-permute-start.1) | collective-permute-done | bytes 800 | tf_op jit(solution)/shard_map/ppermute | solution.py:18
  18.2 0.7 broadcast_compare_fusion
  18.9 39.3 %psum.71 = f32[3]{0:T(128)S(1)} all-reduce(f32[3]{0:T(128)S(1)} %get-tuple-element.24), channel_id=1, replica_groups=mesh['kv'=4,'tp'=8] {'kv','tp'}, use_global_device_ids=true, to_apply=%region_2.4 | all-reduce | flops 3 | bytes 24 | tf_op jit(solution)/shard_map/psum | solution.py:22
  58.2 4.8 %collective-permute-done.3 = bf16[3,128]{1,0:T(4,128)(2,1)S(1)} collective-permute-done((bf16[3,128]{1,0:T(4,128)(2,1)S(1)}, bf16[3,128]{1,0:T(4,128)(2,1)S(1)}, u32[]{:S(2)}, u32[]{:S(2)}) %collective-permute-start.3) | collective-permute-done | bytes 800 | tf_op jit(solution)/shard_map/ppermute | solution.py:18
  63.0 4.8 %collective-permute-done.4 = bf16[3,128]{1,0:T(4,128)(2,1)S(1)} collective-permute-done((bf16[3,128]{1,0:T(4,128)(2,1)S(1)}, bf16[3,128]{1,0:T(4,128)(2,1)S(1)}, u32[]{:S(2)}, u32[]{:S(2)}) %collective-permute-start.4) | collective-permute-done | bytes 800 | tf_op jit(solution)/shard_map/ppermute | solution.py:18
  67.8 4.8 %collective-permute-done.5 = bf16[3,128]{1,0:T(4,128)(2,1)S(1)} collective-permute-done((bf16[3,128]{1,0:T(4,128)(2,1)S(1)}, bf16[3,128]{1,0:T(4,128)(2,1)S(1)}, u32[]{:S(2)}, u32[]{:S(2)}) %collective-permute-start.5) | collective-permute-done | bytes 800 | tf_op jit(solution)/shard_map/ppermute | solution.py:18
  72.6 0.8 dynamic_slice.22
  73.4 1.2 dynamic-slice
  75.3 2.1 collective-permute-done.6
  77.5 1.1 fusion.27
  78.6 1.1 fusion.32
  79.7 1.2 fusion.30
  80.9 1.0 fusion.3
  81.9 10.7 %all-reduce.5 = (f32[3,256]{1,0:T(4,128)S(1)}, f32[3,32]{1,0:T(4,128)S(1)}, f32[3,128]{1,0:T(4,128)S(1)}) all-reduce(f32[3,256]{1,0:T(4,128)S(1)} %fusion.30, f32[3,32]{1,0:T(4,128)S(1)} %fusion.3, f32[3,128]{1,0:T(4,128)S(1)} %fusion.27), channel_id=1, replica_groups=mesh['kv'=4,'tp'=8] {'kv'}, use_global_device_ids=true, to_apply=%region_0.2 | all-reduce | flops 1248 | bytes 9984 | tf_op jit(solution)/shard_map/psum | solution.py:55
  92.9 12.8 %all_gather.3 = bf16[3,2048]{1,0:T(4,128)(2,1)S(1)} all-gather(bf16[3,256]{1,0:T(4,128)(2,1)S(1)} %multiply_convert_fusion.1), channel_id=1, replica_groups=mesh['kv'=4,'tp'=8] {'tp'}, dimensions={1}, use_global_device_ids=true | all-gather | bytes 13824 | tf_op jit(solution)/shard_map/all_gather | solution.py:63
  105.6 0.1 reshape.78
  105.7 0.1 fusion.34
  106.0 1.1 convolution_multiply_fusion
  107.0 0.7 fusion.18
  107.8 1.0 fusion
  108.9 37.8 %pmax.7 = f32[3,32]{1,0:T(4,128)S(1)} all-reduce(f32[3,32]{1,0:T(4,128)S(1)} %max.17), channel_id=1, replica_groups=mesh['kv'=4,'tp'=8] {'kv','tp'}, use_global_device_ids=true, to_apply=%region_6.8 | all-reduce | flops 96 | bytes 768 | tf_op jit(solution)/shard_map/pmax | solution.py:90
  146.7 0.2 fusion.1
  146.9 1.1 fusion.35
  147.9 27.8 %all-reduce.2 = (f32[3,32,64]{2,1,0:T(8,128)}, f32[3,32]{1,0:T(4,128)S(1)}) all-reduce(f32[3,32,64]{2,1,0:T(8,128)S(1)} %bitcast.36, f32[3,32]{1,0:T(4,128)S(1)} %get-tuple-element.22), channel_id=2, replica_groups=mesh['kv'=4,'tp'=8] {'tp'}, use_global_device_ids=true, to_apply=%region_7.9.clone | all-reduce | flops 6240 | bytes 49920
  175.8 0.7 constant_dynamic-slice_fusion.1
  176.5 15.8 %all-reduce.4 = (f32[3,4,64]{2,1,0:T(4,128)S(1)}, f32[3,4]{1,0:T(4,128)S(1)}, f32[3,128]{1,0:T(4,128)S(1)}) all-reduce(f32[3,4,64]{2,1,0:T(4,128)S(1)} %constant_dynamic-slice_fusion.1, f32[3,4]{1,0:T(4,128)S(1)} %constant_dynamic-slice_fusion, f32[3,128]{1,0:T(4,128)S(1)} %fusion.32), channel_id=1, replica_groups=mesh['kv'=4,'tp'=8] {'kv'}, use_global_device_ids=true, to_apply=%region_8.10 | all-reduce | flops 1164 | bytes 9312 | tf_op jit(solution)/shard_map/psum | solution.py:102
  192.6 0.2 multiply_reduce_fusion
  193.0 1.1 convolution_bitcast_fusion.1
  194.2 27.7 %reduce-scatter.9.cloned.1.call-done = f32[128,3]{1,0:T(8,128)} async-done(((f32[1024,3]{1,0:T(8,128)}), f32[128,3]{1,0:T(8,128)}) %reduce-scatter.9.cloned.1.call-update) | async-done | bytes 1552
  221.9 0.9 copy.24
  222.8 0.1 fusion.16
  223.0 4.8 %collective-permute-done.7 = bf16[3,128]{1,0:T(4,128)(2,1)S(1)} collective-permute-done((bf16[3,128]{1,0:T(4,128)(2,1)S(1)}, bf16[3,128]{1,0:T(4,128)(2,1)S(1)}, u32[]{:S(2)}, u32[]{:S(2)}) %collective-permute-start.7) | collective-permute-done | bytes 800 | tf_op jit(solution)/shard_map/ppermute | solution.py:18
  227.8 4.8 %collective-permute-done.8 = bf16[3,128]{1,0:T(4,128)(2,1)S(1)} collective-permute-done((bf16[3,128]{1,0:T(4,128)(2,1)S(1)}, bf16[3,128]{1,0:T(4,128)(2,1)S(1)}, u32[]{:S(2)}, u32[]{:S(2)}) %collective-permute-start.8) | collective-permute-done | bytes 800 | tf_op jit(solution)/shard_map/ppermute | solution.py:18
  232.6 4.8 %collective-permute-done.9 = bf16[3,128]{1,0:T(4,128)(2,1)S(1)} collective-permute-done((bf16[3,128]{1,0:T(4,128)(2,1)S(1)}, bf16[3,128]{1,0:T(4,128)(2,1)S(1)}, u32[]{:S(2)}, u32[]{:S(2)}) %collective-permute-start.9) | collective-permute-done | bytes 800 | tf_op jit(solution)/shard_map/ppermute | solution.py:18
  237.4 4.8 %collective-permute-done.10 = bf16[3,128]{1,0:T(4,128)(2,1)S(1)} collective-permute-done((bf16[3,128]{1,0:T(4,128)(2,1)S(1)}, bf16[3,128]{1,0:T(4,128)(2,1)S(1)}, u32[]{:S(2)}, u32[]{:S(2)}) %collective-permute-start.10) | collective-permute-done | bytes 800 | tf_op jit(solution)/shard_map/ppermute | solution.py:18
  242.2 4.8 %collective-permute-done.11 = bf16[3,128]{1,0:T(4,128)(2,1)S(1)} collective-permute-done((bf16[3,128]{1,0:T(4,128)(2,1)S(1)}, bf16[3,128]{1,0:T(4,128)(2,1)S(1)}, u32[]{:S(2)}, u32[]{:S(2)}) %collective-permute-start.11) | collective-permute-done | bytes 800 | tf_op jit(solution)/shard_map/ppermute | solution.py:18
  247.0 38.8 %psum.78 = f32[3]{0:T(128)S(1)} all-reduce(f32[3]{0:T(128)S(1)} %get-tuple-element.16), channel_id=1, replica_groups=mesh['kv'=4,'tp'=8] {'kv','tp'}, use_global_device_ids=true, to_apply=%region_17.19 | all-reduce | flops 3 | bytes 24 | tf_op jit(solution)/shard_map/psum | solution.py:22
  285.9 4.8 %collective-permute-done.13 = bf16[3,128]{1,0:T(4,128)(2,1)S(1)} collective-permute-done((bf16[3,128]{1,0:T(4,128)(2,1)S(1)}, bf16[3,128]{1,0:T(4,128)(2,1)S(1)}, u32[]{:S(2)}, u32[]{:S(2)}) %collective-permute-start.13) | collective-permute-done | bytes 800 | tf_op jit(solution)/shard_map/ppermute | solution.py:18
  290.8 0.5 fusion.21
  291.2 0.5 fusion.23
  291.7 17.3 %all-reduce.3 = (f32[3,1408]{1,0:T(4,128)S(1)}, f32[3,1408]{1,0:T(4,128)S(1)}) all-reduce(f32[3,1408]{1,0:T(4,128)S(1)} %fusion.23, f32[3,1408]{1,0:T(4,128)S(1)} %fusion.21), channel_id=1, replica_groups=mesh['kv'=4,'tp'=8] {'kv'}, use_global_device_ids=true, to_apply=%region_18.20 | all-reduce | flops 8448 | bytes 67584 | tf_op jit(solution)/shard_map/psum | solution.py:126
  309.1 3.8 %convolution_bitcast_fusion = f32[1024,3]{1,0:T(8,128)} fusion(bf16[1408,1024]{1,0:T(8,128)(2,1)} %param.35, f32[3,1408]{1,0:T(4,128)S(1)} %get-tuple-element.8, f32[3,1408]{1,0:T(4,128)S(1)} %get-tuple-element.9, f32[3]{0:T(128)S(1)} %add_rsqrt_fusion.1), kind=kOutput, calls=%fused_computation | convolution fusion | flops 8684544 | bytes 2929676
  312.9 28.4 %reduce-scatter.11.cloned.1.call-done = f32[128,3]{1,0:T(8,128)} async-done(((f32[1024,3]{1,0:T(8,128)}), f32[128,3]{1,0:T(8,128)}) %reduce-scatter.11.cloned.1.call-update) | async-done | bytes 1552
  341.3 0.9 copy.26
  342.2 0.6 fusion.17
  (65 shorter events, 1.4 us)
Async XLA Ops:
  6.5 284.2 %copy-start = (bf16[1024,1408]{1,0:T(8,128)(2,1)S(1)}, bf16[1024,1408]{1,0:T(8,128)(2,1)}, u32[]{:S(2)}) copy-start(bf16[1024,1408]{1,0:T(8,128)(2,1)} %param.33) | copy-start | bytes 8650756
  6.5 216.3 %copy-start.3 = (bf16[3,128]{1,0:T(4,128)(2,1)S(1)}, bf16[3,128]{1,0:T(4,128)(2,1)}, u32[]{:S(2)}) copy-start(bf16[3,128]{1,0:T(4,128)(2,1)} %param.19) | copy-start | bytes 2308
  6.5 186.4 %copy-start.2 = (bf16[256,1024]{1,0:T(8,128)(2,1)S(1)}, bf16[256,1024]{1,0:T(8,128)(2,1)}, u32[]{:S(2)}) copy-start(bf16[256,1024]{1,0:T(8,128)(2,1)} %param.31) | copy-start | bytes 1572868
  6.5 216.4 %copy-start.4 = (f32[128]{0:T(128)S(1)}, f32[128]{0:T(128)}, u32[]{:S(2)}) copy-start(f32[128]{0:T(128)} %param.32) | copy-start | bytes 1540
  6.5 215.4 %reduce-scatter.9.cloned.1.call-start = ((), (), s32[]{:S(2)}) async-start(), calls=%async_computation.2 | async-start | bytes 589824
  7.6 5.8 %collective-permute-start = (bf16[3,128]{1,0:T(4,128)(2,1)S(1)}, bf16[3,128]{1,0:T(4,128)(2,1)S(1)}, u32[]{:S(2)}, u32[]{:S(2)}) collective-permute-start(bf16[3,128]{1,0:T(4,128)(2,1)S(1)} %get-tuple-element.25), channel_id=1, source_target_pairs={{0,1},{1,2},{2,3},{3,4},{4,5},{5,6},{6,7},{7,0},{8,9},{9,10},{10,1... | collective-permute-start | bytes 2312 | tf_op jit(solution)/shard_map/ppermute | solution.py:18
  13.4 4.8 %collective-permute-start.1 = (bf16[3,128]{1,0:T(4,128)(2,1)S(1)}, bf16[3,128]{1,0:T(4,128)(2,1)S(1)}, u32[]{:S(2)}, u32[]{:S(2)}) collective-permute-start(bf16[3,128]{1,0:T(4,128)(2,1)S(1)} %collective-permute-done), channel_id=1, source_target_pairs={{0,1},{1,2},{2,3},{3,4},{4,5},{5,6},{6,7},{7,0},{8,9},{9,10},{10,1... | collective-permute-start | bytes 2312 | tf_op jit(solution)/shard_map/ppermute | solution.py:18
  18.2 40.0 %collective-permute-start.2 = (bf16[3,128]{1,0:T(4,128)(2,1)S(1)}, bf16[3,128]{1,0:T(4,128)(2,1)S(1)}, u32[]{:S(2)}, u32[]{:S(2)}) collective-permute-start(bf16[3,128]{1,0:T(4,128)(2,1)S(1)} %collective-permute-done.1), channel_id=1, source_target_pairs={{0,1},{1,2},{2,3},{3,4},{4,5},{5,6},{6,7},{7,0},{8,9},{9,10},{10,1... | collective-permute-start | bytes 2312 | tf_op jit(solution)/shard_map/ppermute | solution.py:18
  58.2 4.8 %collective-permute-start.3 = (bf16[3,128]{1,0:T(4,128)(2,1)S(1)}, bf16[3,128]{1,0:T(4,128)(2,1)S(1)}, u32[]{:S(2)}, u32[]{:S(2)}) collective-permute-start(bf16[3,128]{1,0:T(4,128)(2,1)S(1)} %collective-permute-done.2), channel_id=1, source_target_pairs={{0,1},{1,2},{2,3},{3,4},{4,5},{5,6},{6,7},{7,0},{8,9},{9,10},{10,1... | collective-permute-start | bytes 2312 | tf_op jit(solution)/shard_map/ppermute | solution.py:18
  63.0 4.8 %collective-permute-start.4 = (bf16[3,128]{1,0:T(4,128)(2,1)S(1)}, bf16[3,128]{1,0:T(4,128)(2,1)S(1)}, u32[]{:S(2)}, u32[]{:S(2)}) collective-permute-start(bf16[3,128]{1,0:T(4,128)(2,1)S(1)} %collective-permute-done.3), channel_id=1, source_target_pairs={{0,1},{1,2},{2,3},{3,4},{4,5},{5,6},{6,7},{7,0},{8,9},{9,10},{10,1... | collective-permute-start | bytes 2312 | tf_op jit(solution)/shard_map/ppermute | solution.py:18
  67.8 4.8 %collective-permute-start.5 = (bf16[3,128]{1,0:T(4,128)(2,1)S(1)}, bf16[3,128]{1,0:T(4,128)(2,1)S(1)}, u32[]{:S(2)}, u32[]{:S(2)}) collective-permute-start(bf16[3,128]{1,0:T(4,128)(2,1)S(1)} %collective-permute-done.4), channel_id=1, source_target_pairs={{0,1},{1,2},{2,3},{3,4},{4,5},{5,6},{6,7},{7,0},{8,9},{9,10},{10,1... | collective-permute-start | bytes 2312 | tf_op jit(solution)/shard_map/ppermute | solution.py:18
  72.6 4.8 %collective-permute-start.6 = (bf16[3,128]{1,0:T(4,128)(2,1)S(1)}, bf16[3,128]{1,0:T(4,128)(2,1)S(1)}, u32[]{:S(2)}, u32[]{:S(2)}) collective-permute-start(bf16[3,128]{1,0:T(4,128)(2,1)S(1)} %collective-permute-done.5), channel_id=1, source_target_pairs={{0,1},{1,2},{2,3},{3,4},{4,5},{5,6},{6,7},{7,0},{8,9},{9,10},{10,1... | collective-permute-start | bytes 2312 | tf_op jit(solution)/shard_map/ppermute | solution.py:18
  194.1 147.2 %reduce-scatter.11.cloned.1.call-start = ((), (), s32[]{:S(2)}) async-start(), calls=%async_computation.3 | async-start | bytes 589824
  223.0 4.8 %collective-permute-start.7 = (bf16[3,128]{1,0:T(4,128)(2,1)S(1)}, bf16[3,128]{1,0:T(4,128)(2,1)S(1)}, u32[]{:S(2)}, u32[]{:S(2)}) collective-permute-start(bf16[3,128]{1,0:T(4,128)(2,1)S(1)} %fusion.15), channel_id=1, source_target_pairs={{0,1},{1,2},{2,3},{3,4},{4,5},{5,6},{6,7},{7,0},{8,9},{9,10},{10,1... | collective-permute-start | bytes 2312 | tf_op jit(solution)/shard_map/ppermute | solution.py:18
  227.8 4.8 %collective-permute-start.8 = (bf16[3,128]{1,0:T(4,128)(2,1)S(1)}, bf16[3,128]{1,0:T(4,128)(2,1)S(1)}, u32[]{:S(2)}, u32[]{:S(2)}) collective-permute-start(bf16[3,128]{1,0:T(4,128)(2,1)S(1)} %collective-permute-done.7), channel_id=1, source_target_pairs={{0,1},{1,2},{2,3},{3,4},{4,5},{5,6},{6,7},{7,0},{8,9},{9,10},{10,1... | collective-permute-start | bytes 2312 | tf_op jit(solution)/shard_map/ppermute | solution.py:18
  232.6 4.8 %collective-permute-start.9 = (bf16[3,128]{1,0:T(4,128)(2,1)S(1)}, bf16[3,128]{1,0:T(4,128)(2,1)S(1)}, u32[]{:S(2)}, u32[]{:S(2)}) collective-permute-start(bf16[3,128]{1,0:T(4,128)(2,1)S(1)} %collective-permute-done.8), channel_id=1, source_target_pairs={{0,1},{1,2},{2,3},{3,4},{4,5},{5,6},{6,7},{7,0},{8,9},{9,10},{10,1... | collective-permute-start | bytes 2312 | tf_op jit(solution)/shard_map/ppermute | solution.py:18
  237.4 4.8 %collective-permute-start.10 = (bf16[3,128]{1,0:T(4,128)(2,1)S(1)}, bf16[3,128]{1,0:T(4,128)(2,1)S(1)}, u32[]{:S(2)}, u32[]{:S(2)}) collective-permute-start(bf16[3,128]{1,0:T(4,128)(2,1)S(1)} %collective-permute-done.9), channel_id=1, source_target_pairs={{0,1},{1,2},{2,3},{3,4},{4,5},{5,6},{6,7},{7,0},{8,9},{9,10},{10,1... | collective-permute-start | bytes 2312 | tf_op jit(solution)/shard_map/ppermute | solution.py:18
  242.2 4.8 %collective-permute-start.11 = (bf16[3,128]{1,0:T(4,128)(2,1)S(1)}, bf16[3,128]{1,0:T(4,128)(2,1)S(1)}, u32[]{:S(2)}, u32[]{:S(2)}) collective-permute-start(bf16[3,128]{1,0:T(4,128)(2,1)S(1)} %collective-permute-done.10), channel_id=1, source_target_pairs={{0,1},{1,2},{2,3},{3,4},{4,5},{5,6},{6,7},{7,0},{8,9},{9,10},{10,1... | collective-permute-start | bytes 2312 | tf_op jit(solution)/shard_map/ppermute | solution.py:18
  247.0 38.8 %collective-permute-start.12 = (bf16[3,128]{1,0:T(4,128)(2,1)S(1)}, bf16[3,128]{1,0:T(4,128)(2,1)S(1)}, u32[]{:S(2)}, u32[]{:S(2)}) collective-permute-start(bf16[3,128]{1,0:T(4,128)(2,1)S(1)} %collective-permute-done.11), channel_id=1, source_target_pairs={{0,1},{1,2},{2,3},{3,4},{4,5},{5,6},{6,7},{7,0},{8,9},{9,10},{10,1... | collective-permute-start | bytes 2312 | tf_op jit(solution)/shard_map/ppermute | solution.py:18
  285.8 5.4 %copy-start.1 = (bf16[1024,1408]{1,0:T(8,128)(2,1)S(1)}, bf16[1024,1408]{1,0:T(8,128)(2,1)}, u32[]{:S(2)}) copy-start(bf16[1024,1408]{1,0:T(8,128)(2,1)} %param.34) | copy-start | bytes 8650756
  285.8 4.8 %collective-permute-start.13 = (bf16[3,128]{1,0:T(4,128)(2,1)S(1)}, bf16[3,128]{1,0:T(4,128)(2,1)S(1)}, u32[]{:S(2)}, u32[]{:S(2)}) collective-permute-start(bf16[3,128]{1,0:T(4,128)(2,1)S(1)} %collective-permute-done.12), channel_id=1, source_target_pairs={{0,1},{1,2},{2,3},{3,4},{4,5},{5,6},{6,7},{7,0},{8,9},{9,10},{10,1... | collective-permute-start | bytes 2312 | tf_op jit(solution)/shard_map/ppermute | solution.py:18
Sparse Core Ops, SparseCore 0:
  194.2 27.6 reduce-scatter.8
  313.1 28.2 reduce-scatter.10
